TPU v7x, 32 devices: a whole 2x2x4 slice. The times are simulated.
32 devices in a mesh: ep: 8 (over z, core), tp: 4 (over y, x).
Axes of the slice: x: 2, y: 2, z: 4, core: 2. Of those that a mesh axis runs over, the one named last changes fastest.
Arguments:
- query_rows: bfloat16 [3072, 2048], P('ep', 'tp'), may hold values from -6 to 6
- key_rows: bfloat16 [3072, 2048], P('ep', 'tp'), may hold values from -6 to 6
- value_rows: bfloat16 [3072, 2048], P('ep', 'tp'), may hold values from -6 to 6
- second_scale: float32 [16], P('tp'), may hold values from 0.3 to 0.8
- head_gain: float32 [128], replicated, may hold values from 0.1 to 1.9
- out_weight: bfloat16 [2048, 4096], P(None, 'tp'), may hold values from -0.125 to 0.125
- routed_rows: bfloat16 [1024, 4096], P('ep', 'tp'), may hold values from -6 to 6
- norm_gain: float32 [4096], replicated, may hold values from 0.1 to 1.9
- route_ids: int32 [1024, 2], P('ep'), may hold values from 0 to 7, all different within a row; in each aligned block of 128 rows (0 to 127, 128 to 255, ...) at most 64 rows name the same one
- route_weight: float32 [1024, 2], P('ep'), may hold values from 0.1 to 0.9
- expert_gate: bfloat16 [8, 4096, 2048], P('ep', None, 'tp'), may hold values from -0.09375 to 0.09375
- expert_up: bfloat16 [8, 4096, 2048], P('ep', None, 'tp'), may hold values from -0.09375 to 0.09375
- expert_down: bfloat16 [8, 2048, 4096], P('ep', None, 'tp'), may hold values from -0.125 to 0.125
Outputs:
- mixer_out: bfloat16 [3072, 4096], P('ep', 'tp')
- expert_mix: bfloat16 [1024, 4096], P('ep', 'tp')
Inputs may be any that keep to these rules, and one draw needn't show every extreme that they name: `route_ids`: among the 128 tokens of one index of ep, no expert is named by more than 64 of them, a bound that some block reaches.
All inputs are finite; a program needn't handle non-finite values.
Results may differ from a plain program's by a relative error of at most 0.0085.
Values may be sent and summed in bfloat16 or wider, within the bound.
No kernel may reach another device: no remote copies, remote signals or barrier semaphores. Data moves between devices by JAX's collectives and lax.ppermute only.
A program may use at most 128 MiB of HBM per device.

v0:
```python
import jax
import jax.numpy as jnp
from jax import lax
from jax.sharding import PartitionSpec as P

eps = 1e-06
head_factor = 0.8
neg_big = -1e30
key_block_rows = 1024


def rms_rows(rows_in, gain):
    floats = rows_in.astype(jnp.float32)
    factor = lax.rsqrt(jnp.mean(floats * floats, axis=-1, keepdims=True) + eps)
    return (floats * factor * gain).astype(jnp.bfloat16)


def per_device(
    query_rows,
    key_rows,
    value_rows,
    second_scale,
    head_gain,
    out_weight,
    routed_rows,
    norm_gain,
    route_ids,
    route_weight,
    expert_gate,
    expert_up,
    expert_down,
):
    count_a = query_rows.shape[0]
    per_head = second_scale.shape[0]
    head_dim = query_rows.shape[1] // (2 * per_head)
    value_dim = head_gain.shape[0]
    query_four = query_rows.reshape(count_a, per_head, 2, head_dim)
    query_pos = lax.axis_index("ep") * count_a + jnp.arange(count_a, dtype=jnp.int32)

    def key_block(carry_state, key_part, value_part, block_start):
        key_count = key_part.shape[0]
        key_four = key_part.reshape(key_count, per_head, 2, head_dim)
        value_three = value_part.reshape(key_count, per_head, value_dim)
        scores = jnp.einsum(
            "ihcd,jhcd->ihcj", query_four, key_four, preferred_element_type=jnp.float32
        ) * head_dim ** (-0.5)
        allowed = (
            query_pos[:, None] >= block_start + jnp.arange(key_count, dtype=jnp.int32)[None, :]
        )[:, None, None, :]
        scores = jnp.where(allowed, scores, neg_big)
        old_max, old_sum, old_acc = carry_state
        new_max = jnp.maximum(old_max, jnp.max(scores, axis=-1))
        weights = jnp.where(allowed, jnp.exp(scores - new_max[..., None]), 0.0)
        shrink = jnp.exp(old_max - new_max)
        new_sum = old_sum * shrink + jnp.sum(weights, axis=-1)
        update = jnp.einsum(
            "ihcj,jhe->ihce",
            weights.astype(jnp.bfloat16),
            value_three,
            preferred_element_type=jnp.float32,
        )
        return (new_max, new_sum, old_acc * shrink[..., None] + update)

    start_state = (
        jnp.full((count_a, per_head, 2), neg_big, jnp.float32),
        jnp.zeros((count_a, per_head, 2), jnp.float32),
        jnp.zeros((count_a, per_head, 2, value_dim), jnp.float32),
    )
    key_part = lax.all_gather(key_rows, "ep", axis=0, tiled=True)
    value_part = lax.all_gather(value_rows, "ep", axis=0, tiled=True)
    key_count = key_part.shape[0]

    def step_block(block_num, inner_state):
        offset_rows = block_num * key_block_rows
        key_slice = lax.dynamic_slice_in_dim(key_part, offset_rows, key_block_rows, 0)
        value_slice = lax.dynamic_slice_in_dim(value_part, offset_rows, key_block_rows, 0)
        return key_block(inner_state, key_slice, value_slice, offset_rows)

    run_max, run_sum, run_acc = lax.fori_loop(
        0, key_count // key_block_rows, step_block, start_state
    )
    maps_both = run_acc / run_sum[..., None]
    mixed_maps = maps_both[:, :, 0] - second_scale[None, :, None] * maps_both[:, :, 1]
    mean_sq = jnp.mean(mixed_maps * mixed_maps, axis=-1, keepdims=True)
    head_out = (
        (mixed_maps * lax.rsqrt(mean_sq + eps) * head_gain * head_factor)
        .astype(jnp.bfloat16)
        .reshape(count_a, per_head * value_dim)
    )
    count_b = routed_rows.shape[0]
    route_count = route_ids.shape[1]
    experts_here = expert_gate.shape[0]
    ep_devices = lax.axis_size("ep")
    expert_total = experts_here * ep_devices
    capacity = 2 * count_b * route_count // expert_total
    flat_expert = route_ids.reshape(-1)
    chosen = (flat_expert[:, None] == jnp.arange(expert_total, dtype=jnp.int32)[None, :]).astype(
        jnp.int32
    )
    ranks = jnp.sum((jnp.cumsum(chosen, axis=0) - 1) * chosen, axis=1)
    slot_of = flat_expert * capacity + ranks
    token_of = jnp.arange(count_b * route_count, dtype=jnp.int32) // route_count
    slot_token = jnp.full((expert_total * capacity,), count_b, jnp.int32).at[slot_of].set(token_of)
    padded = jnp.concatenate(
        [routed_rows, jnp.zeros((1, routed_rows.shape[1]), jnp.bfloat16)], axis=0
    )
    outgoing = padded[slot_token].reshape(ep_devices, experts_here, capacity, routed_rows.shape[1])
    column_parts = lax.all_to_all(outgoing, "ep", split_axis=0, concat_axis=0, tiled=True)
    arrived = rms_rows(lax.all_gather(column_parts, "tp", axis=3, tiled=True), norm_gain)
    gate_val = jnp.einsum(
        "sxcd,xdf->sxcf", arrived, expert_gate, preferred_element_type=jnp.float32
    )
    up_val = jnp.einsum("sxcd,xdf->sxcf", arrived, expert_up, preferred_element_type=jnp.float32)
    hidden = (jax.nn.silu(gate_val) * up_val).astype(jnp.bfloat16)
    weight_rows = out_weight
    attn_total = jnp.dot(
        lax.all_gather(
            head_out.reshape(1, 1, count_a, head_out.shape[1]), "tp", axis=3, tiled=True
        )[0, 0],
        weight_rows,
        preferred_element_type=jnp.float32,
    )
    weight_rows = expert_down
    moe_total = jnp.einsum(
        "sxcf,xfd->sxcd",
        lax.all_gather(hidden, "tp", axis=3, tiled=True),
        weight_rows,
        preferred_element_type=jnp.float32,
    )
    mixer_out = attn_total.astype(jnp.bfloat16)
    returned = lax.all_to_all(
        moe_total.astype(jnp.bfloat16), "ep", split_axis=0, concat_axis=0, tiled=True
    )
    flat_back = returned.reshape(expert_total * capacity, returned.shape[3])
    picked = flat_back[slot_of].astype(jnp.float32).reshape(count_b, route_count, returned.shape[3])
    expert_mix = jnp.sum(picked * route_weight[:, :, None], axis=1).astype(jnp.bfloat16)
    return (mixer_out, expert_mix)


def solution(mesh):
    placed = (
        P("ep", "tp"),
        P("ep", "tp"),
        P("ep", "tp"),
        P("tp"),
        P(),
        P(None, "tp"),
        P("ep", "tp"),
        P(),
        P("ep", None),
        P("ep", None),
        P("ep", None, "tp"),
        P("ep", None, "tp"),
        P("ep", None, "tp"),
    )
    return jax.shard_map(
        per_device,
        mesh=mesh,
        in_specs=placed,
        out_specs=(P("ep", "tp"), P("ep", "tp")),
        check_vma=False,
    )
```

profile of v0, /device:TPU:0, one launch (start us, length us, event | category | flops | bytes accessed | tf_op | source)
XLA Modules:
  0.0 287.7 jit_solution(6418652989304294273)
XLA Ops:
  10.2 1.4 scatter_custom_fusion
  12.6 2.1 gather_fusion
  14.7 33.0 %all_to_all.10 = bf16[8,1,64,1024]{3,2,1,0:T(8,128)(2,1)} all-to-all(bf16[8,1,64,1024]{3,2,1,0:T(8,128)(2,1)S(1)} %bitcast.152), channel_id=1, replica_groups=mesh['ep'=8,'tp'=4] {'ep'}, dimensions={0} | all-to-all | bytes 2097152 | tf_op jit(solution)/shard_map/all_to_all | solution.py:108
  49.8 1.2 copy.32
  51.1 48.2 %all-gather.12.cloned.1.call-done = bf16[8,1,64,4096]{3,2,1,0:T(8,128)(2,1)} async-done(((bf16[8,1,64,1024]{3,2,1,0:T(8,128)(2,1)}), bf16[8,1,64,4096]{3,2,1,0:T(8,128)(2,1)}) %all-gather.12.cloned.1.call-update) | async-done | bytes 4194320 | tf_op jit(solution)/shard_map/all_gather | solution.py:109
  99.4 3.2 %fusion.15 = f32[8,64]{1,0:T(8,128)S(1)} fusion(bf16[8,1,64,4096]{3,2,1,0:T(8,128)(2,1)} %all-gather.12.cloned.1.call-done), kind=kLoop, calls=%fused_computation.28 | loop fusion | flops 6290944 | bytes 4196352 | tf_op jit(solution)/shard_map/reduce_sum | solution.py:14
  102.8 4.7 %fusion.43 = f32[8,1,64,512]{3,2,0,1:T(8,128)S(1)} fusion(bf16[1,4096,512]{2,1,0:T(8,128)(2,1)} %param.25, bf16[8,1,64,4096]{3,2,1,0:T(8,128)(2,1)S(1)} %copy-done.1, f32[4096]{0:T(1024)S(1)} %copy-done.8, f32[8,64]{1,0:T(8,128)S(1)} %add_rsqrt_fusion.1), kind=kOutput, calls=%fused_computation.44 | convolution fusion | flops 2155872256 | bytes 9455616 | tf_op jit(solution)/shard_map/sxcd,xdf->sxcf/dot_general | solution.py:110
  107.5 3.3 %fusion.58 = bf16[8,1,64,512]{3,2,0,1:T(8,128)(2,1)} fusion(bf16[1,4096,512]{2,1,0:T(8,128)(2,1)S(1)} %copy-done.7, bf16[8,1,64,4096]{3,2,1,0:T(8,128)(2,1)S(1)} %copy-done.1, f32[4096]{0:T(1024)S(1)} %copy-done.8, f32[8,64]{1,0:T(8,128)S(1)} %add_rsqrt_fusion.1, f32[8,1,64,512]{3,2,0,1:T(8,128)S(1)} %fusion.43), kind=kOutput, calls=%fused_computation.47 | convolution fusion | flops 2157445120 | bytes 9979904 | tf_op jit(solution)/shard_map/sxcd,xdf->sxcf/dot_general | solution.py:113
  111.0 27.7 %all-gather.6.cloned.1.call-done = bf16[3072,512]{0,1:T(8,128)(2,1)} async-done(((bf16[384,512]{0,1:T(8,128)(2,1)}), bf16[3072,512]{0,1:T(8,128)(2,1)}) %all-gather.6.cloned.1.call-update) | async-done | bytes 3145744 | tf_op jit(solution)/shard_map/all_gather | solution.py:69
  138.8 38.8 %all-gather.8.cloned.1.call-done = bf16[3072,512]{0,1:T(8,128)(2,1)} async-done(((bf16[384,512]{0,1:T(8,128)(2,1)}), bf16[3072,512]{0,1:T(8,128)(2,1)}) %all-gather.8.cloned.1.call-update) | async-done | bytes 3145744 | tf_op jit(solution)/shard_map/all_gather | solution.py:70
  177.5 61.9 %while.18 = (s32[]{:T(128)}, f32[384,4,2]{0,2,1:T(2,128)S(1)}, f32[384,4,2]{0,2,1:T(2,128)S(1)}, f32[384,4,2,128]{0,3,2,1:T(8,128)S(1)}, bf16[3072,512]{0,1:T(8,...) while((s32[]{:T(128)}, f32[384,4,2]{0,2,1:T(2,128)S(1)}, ...), condition=%wide.region_3.4_spmd.clone, body=%wide.region_0.3_spmd.clone.sunk | while | flops 1250443648 | bytes 99691744 | solution.py:79
  177.8 1.7 constant_dynamic-slice_fusion.3
  179.5 6.7 %fusion.86 = (f32[384,4,2]{0,2,1:T(2,128)S(1)}, f32[4,2,1024,384]{3,2,1,0:T(8,128)}) fusion(pred[384,1024]{0,1:T(8,128)(4,1)S(1)} %broadcast_compare_fusion.2, bf16[1024,4,2,64]{0,3,2,1:T(8,128)(2,1)S(1)} %bitcast.148, bf16[384,4,2,64]{0,3,2,1:T(8,128)(2,1)S(1)} %get-tuple-element.290), kind=kOutput, calls=%fused_computation.6.clone.1 | convolution fusion | flops 412087296 | bytes 14430208 | tf_op jit(solution)/shard_map/while/body/eval_jaxpr/ihcd,jhcd->ihcj/dot_general | solution.py:44
  186.2 7.0 %fusion.88 = f32[384,4,2]{0,2,1:T(2,128)S(1)} fusion(f32[4,2,1024,384]{3,2,1,0:T(8,128)} %get-tuple-element.257, f32[384,4,2]{0,2,1:T(2,128)S(1)} %fusion.87, pred[384,1024]{0,1:T(8,128)(4,1)S(1)} %broadcast_compare_fusion.2), kind=kLoop, calls=%fused_computation.8.clone.1 | loop fusion | flops 15725568 | bytes 13000704 | tf_op jit(solution)/shard_map/while/body/eval_jaxpr/reduce_sum | solution.py:55
  193.2 1.5 copy-done
  194.7 3.6 %bitcast_add_fusion.2 = f32[384,4,2,128]{0,3,2,1:T(8,128)S(1)} fusion(f32[384,4,2,128]{0,3,2,1:T(8,128)S(1)} %get-tuple-element.276, bf16[1024,4,128,1]{0,2,3,1:T(8,128)(2,1)S(1)} %bitcast.149, f32[4,2,1024,384]{3,2,1,0:T(8,128)S(1)} %copy-done, f32[384,4,2]{0,2,1:T(2,128)S(1)} %fusion.87, pred[384,1024]{0,1:T(8,128)(4,1)S(1)} %broadcast_compare_fusion.2, ...), kind=kOutput, calls=%fused_computation.11.clone.1 | convolution fusion | flops 822214656 | bytes 17195008 | tf_op jit(solution)/shard_map/while/body/eval_jaxpr/ihcj,jhe->ihce/dot_general | solution.py:56
  198.6 1.7 constant_dynamic-slice_fusion.3
  200.3 6.7 %fusion.86 = (f32[384,4,2]{0,2,1:T(2,128)S(1)}, f32[4,2,1024,384]{3,2,1,0:T(8,128)}) fusion(pred[384,1024]{0,1:T(8,128)(4,1)S(1)} %broadcast_compare_fusion.2, bf16[1024,4,2,64]{0,3,2,1:T(8,128)(2,1)S(1)} %bitcast.148, bf16[384,4,2,64]{0,3,2,1:T(8,128)(2,1)S(1)} %get-tuple-element.290), kind=kOutput, calls=%fused_computation.6.clone.1 | convolution fusion | flops 412087296 | bytes 14430208 | tf_op jit(solution)/shard_map/while/body/eval_jaxpr/ihcd,jhcd->ihcj/dot_general | solution.py:44
  207.0 6.8 %fusion.88 = f32[384,4,2]{0,2,1:T(2,128)S(1)} fusion(f32[4,2,1024,384]{3,2,1,0:T(8,128)} %get-tuple-element.257, f32[384,4,2]{0,2,1:T(2,128)S(1)} %fusion.87, pred[384,1024]{0,1:T(8,128)(4,1)S(1)} %broadcast_compare_fusion.2), kind=kLoop, calls=%fused_computation.8.clone.1 | loop fusion | flops 15725568 | bytes 13000704 | tf_op jit(solution)/shard_map/while/body/eval_jaxpr/reduce_sum | solution.py:55
  213.9 1.4 copy-done
  215.3 3.6 %bitcast_add_fusion.2 = f32[384,4,2,128]{0,3,2,1:T(8,128)S(1)} fusion(f32[384,4,2,128]{0,3,2,1:T(8,128)S(1)} %get-tuple-element.276, bf16[1024,4,128,1]{0,2,3,1:T(8,128)(2,1)S(1)} %bitcast.149, f32[4,2,1024,384]{3,2,1,0:T(8,128)S(1)} %copy-done, f32[384,4,2]{0,2,1:T(2,128)S(1)} %fusion.87, pred[384,1024]{0,1:T(8,128)(4,1)S(1)} %broadcast_compare_fusion.2, ...), kind=kOutput, calls=%fused_computation.11.clone.1 | convolution fusion | flops 822214656 | bytes 17195008 | tf_op jit(solution)/shard_map/while/body/eval_jaxpr/ihcj,jhe->ihce/dot_general | solution.py:56
  219.2 1.7 constant_dynamic-slice_fusion.3
  220.9 6.7 %fusion.86 = (f32[384,4,2]{0,2,1:T(2,128)S(1)}, f32[4,2,1024,384]{3,2,1,0:T(8,128)}) fusion(pred[384,1024]{0,1:T(8,128)(4,1)S(1)} %broadcast_compare_fusion.2, bf16[1024,4,2,64]{0,3,2,1:T(8,128)(2,1)S(1)} %bitcast.148, bf16[384,4,2,64]{0,3,2,1:T(8,128)(2,1)S(1)} %get-tuple-element.290), kind=kOutput, calls=%fused_computation.6.clone.1 | convolution fusion | flops 412087296 | bytes 14430208 | tf_op jit(solution)/shard_map/while/body/eval_jaxpr/ihcd,jhcd->ihcj/dot_general | solution.py:44
  227.6 6.8 %fusion.88 = f32[384,4,2]{0,2,1:T(2,128)S(1)} fusion(f32[4,2,1024,384]{3,2,1,0:T(8,128)} %get-tuple-element.257, f32[384,4,2]{0,2,1:T(2,128)S(1)} %fusion.87, pred[384,1024]{0,1:T(8,128)(4,1)S(1)} %broadcast_compare_fusion.2), kind=kLoop, calls=%fused_computation.8.clone.1 | loop fusion | flops 15725568 | bytes 13000704 | tf_op jit(solution)/shard_map/while/body/eval_jaxpr/reduce_sum | solution.py:55
  234.4 1.4 copy-done
  235.9 3.6 %bitcast_add_fusion.2 = f32[384,4,2,128]{0,3,2,1:T(8,128)S(1)} fusion(f32[384,4,2,128]{0,3,2,1:T(8,128)S(1)} %get-tuple-element.276, bf16[1024,4,128,1]{0,2,3,1:T(8,128)(2,1)S(1)} %bitcast.149, f32[4,2,1024,384]{3,2,1,0:T(8,128)S(1)} %copy-done, f32[384,4,2]{0,2,1:T(2,128)S(1)} %fusion.87, pred[384,1024]{0,1:T(8,128)(4,1)S(1)} %broadcast_compare_fusion.2, ...), kind=kOutput, calls=%fused_computation.11.clone.1 | convolution fusion | flops 822214656 | bytes 17195008 | tf_op jit(solution)/shard_map/while/body/eval_jaxpr/ihcj,jhe->ihce/dot_general | solution.py:56
  241.0 6.1 %fusion.38 = bf16[8,1,64,1024]{3,2,1,0:T(8,128)(2,1)} fusion(bf16[1,2048,1024]{2,1,0:T(8,128)(2,1)} %param.27, bf16[8,1,64,2048]{3,2,0,1:T(8,128)(2,1)} %all-gather.14.cloned.1.call-done), kind=kOutput, calls=%fused_computation.43 | convolution fusion | flops 2148007936 | bytes 7340032 | tf_op jit(solution)/shard_map/sxcf,xfd->sxcd/dot_general | solution.py:124
  247.2 3.6 %all-to-all-start.1 = ((bf16[8,1,64,1024]{3,2,1,0:T(8,128)(2,1)}), bf16[8,1,64,1024]{3,2,1,0:T(8,128)(2,1)S(1)}, u32[]{:S(2)}, u32[]{:S(2)}) async-start(bf16[8,1,64,1024]{3,2,1,0:T(8,128)(2,1)} %fusion.38), calls=%async_computation.1 | async-start | bytes 2097152 | tf_op jit(solution)/shard_map/all_to_all | solution.py:131
  250.9 20.8 %all-gather.10.cloned.1.call-done = bf16[1,1,384,2048]{2,3,1,0:T(8,128)(2,1)} async-done(((bf16[1,1,384,512]{2,3,1,0:T(8,128)(2,1)}), bf16[1,1,384,2048]{2,3,1,0:T(8,128)(2,1)}) %all-gather.10.cloned.1.call-update) | async-done | bytes 1572880 | tf_op jit(solution)/shard_map/all_gather | solution.py:117
  271.6 5.4 %fusion.35 = bf16[384,1024]{1,0:T(8,128)(2,1)} fusion(bf16[2048,1024]{1,0:T(8,128)(2,1)} %param.20, bf16[1,1,384,2048]{2,3,1,0:T(8,128)(2,1)} %all-gather.10.cloned.1.call-done), kind=kOutput, calls=%fused_computation.42 | convolution fusion | flops 1611005952 | bytes 6553600 | tf_op jit(solution)/shard_map/dot_general | solution.py:116
  277.2 1.2 gather_fusion.1
  279.0 2.1 multiply_reduce_fusion
  (82 shorter events, 10.1 us)
Async XLA Ops:
  7.2 92.2 %all-gather.12.cloned.1.call-start = ((), (), s32[]{:S(2)}) async-start(), calls=%async_computation.5 | async-start | bytes 5242880 | tf_op jit(solution)/shard_map/all_gather | solution.py:109
  12.6 35.1 %copy-start.2 = (bf16[384,512]{1,0:T(8,128)(2,1)S(1)}, bf16[384,512]{1,0:T(8,128)(2,1)}, u32[]{:S(2)}) copy-start(bf16[384,512]{1,0:T(8,128)(2,1)} %param.16) | copy-start | bytes 1179652
  14.7 34.1 %copy-start.3 = (bf16[384,512]{1,0:T(8,128)(2,1)S(1)}, bf16[384,512]{1,0:T(8,128)(2,1)}, u32[]{:S(2)}) copy-start(bf16[384,512]{1,0:T(8,128)(2,1)} %param.17) | copy-start | bytes 1179652
  14.7 36.3 %copy-start.4 = (f32[4]{0:T(128)S(1)}, f32[4]{0:T(128)}, u32[]{:S(2)}) copy-start(f32[4]{0:T(128)} %param.18) | copy-start | bytes 52
  14.7 36.3 %copy-start.6 = (f32[128]{0:T(128)S(1)}, f32[128]{0:T(128)}, u32[]{:S(2)}) copy-start(f32[128]{0:T(128)} %param.19) | copy-start | bytes 1540
  47.7 54.9 %copy-start.8 = (f32[4096]{0:T(1024)S(1)}, f32[4096]{0:T(1024)}, u32[]{:S(2)}) copy-start(f32[4096]{0:T(1024)} %param.22) | copy-start | bytes 49156
  47.7 91.1 %all-gather.6.cloned.1.call-start = ((), (), s32[]{:S(2)}) async-start(), calls=%async_computation.2 | async-start | bytes 3538944 | tf_op jit(solution)/shard_map/all_gather | solution.py:69
  48.7 128.8 %all-gather.8.cloned.1.call-start = ((), (), s32[]{:S(2)}) async-start(), calls=%async_computation.3 | async-start | bytes 3538944 | tf_op jit(solution)/shard_map/all_gather | solution.py:70
  49.7 191.3 %all-gather.14.cloned.1.call-start = ((), (), s32[]{:S(2)}) async-start(), calls=%async_computation.6 | async-start | bytes 2621440 | tf_op jit(solution)/shard_map/all_gather | solution.py:126
  99.3 3.4 %copy-start.1 = (bf16[8,1,64,4096]{3,2,1,0:T(8,128)(2,1)S(1)}, bf16[8,1,64,4096]{3,2,1,0:T(8,128)(2,1)}, u32[]{:S(2)}) copy-start(bf16[8,1,64,4096]{3,2,1,0:T(8,128)(2,1)} %all-gather.12.cloned.1.call-done) | copy-start | bytes 12582916
  102.8 4.7 %copy-start.7 = (bf16[1,4096,512]{2,1,0:T(8,128)(2,1)S(1)}, bf16[1,4096,512]{2,1,0:T(8,128)(2,1)}, u32[]{:S(2)}) copy-start(bf16[1,4096,512]{2,1,0:T(8,128)(2,1)} %param.26) | copy-start | bytes 12582916
  110.8 160.8 %all-gather.10.cloned.1.call-start = ((), (), s32[]{:S(2)}) async-start(), calls=%async_computation.4 | async-start | bytes 1966080 | tf_op jit(solution)/shard_map/all_gather | solution.py:117
  186.2 8.5 %copy-start = (f32[4,2,1024,384]{3,2,1,0:T(8,128)S(1)}, f32[4,2,1024,384]{3,2,1,0:T(8,128)}, u32[]{:S(2)}) copy-start(f32[4,2,1024,384]{3,2,1,0:T(8,128)} %get-tuple-element.257) | copy-start | bytes 37748740 | tf_op jit(solution)/shard_map/while
  207.0 8.3 %copy-start = (f32[4,2,1024,384]{3,2,1,0:T(8,128)S(1)}, f32[4,2,1024,384]{3,2,1,0:T(8,128)}, u32[]{:S(2)}) copy-start(f32[4,2,1024,384]{3,2,1,0:T(8,128)} %get-tuple-element.257) | copy-start | bytes 37748740 | tf_op jit(solution)/shard_map/while
  227.6 8.3 %copy-start = (f32[4,2,1024,384]{3,2,1,0:T(8,128)S(1)}, f32[4,2,1024,384]{3,2,1,0:T(8,128)}, u32[]{:S(2)}) copy-start(f32[4,2,1024,384]{3,2,1,0:T(8,128)} %get-tuple-element.257) | copy-start | bytes 37748740 | tf_op jit(solution)/shard_map/while
  241.0 9.7 %copy-start.5 = (f32[128,2]{0,1:T(2,128)S(1)}, f32[128,2]{0,1:T(2,128)}, u32[]{:S(2)}) copy-start(f32[128,2]{0,1:T(2,128)} %param.24) | copy-start | bytes 3076
  247.2 30.1 %all-to-all-start.1 = ((bf16[8,1,64,1024]{3,2,1,0:T(8,128)(2,1)}), bf16[8,1,64,1024]{3,2,1,0:T(8,128)(2,1)S(1)}, u32[]{:S(2)}, u32[]{:S(2)}) async-start(bf16[8,1,64,1024]{3,2,1,0:T(8,128)(2,1)} %fusion.38), calls=%async_computation.1 | async-start | bytes 2097152 | tf_op jit(solution)/shard_map/all_to_all | solution.py:131
Sparse Core Ops, SparseCore 0:
  47.8 51.4 all-gather.11
  101.0 37.7 all-gather.5
  140.4 37.0 all-gather.7
  179.8 34.3 all-gather.13
  241.1 30.4 all-gather.9
where the time goes:
time: 288 us
  waiting for transfers between devices  136 us (47%)
  matrix products  50.1 us (17%)
  blocking collectives  33 us (11%)
  other arithmetic  29.5 us (10%)
  local copies, waits for them, and re-layouts  21 us (7%)
  between operations  14 us (5%)
  starting transfers between devices  3.94 us (1%)
    all_gather x1, waiting for transfers between devices, per_device(): lax.all_gather(column_parts, 'tp', axis=3, tiled=True)  48.2 us
    all_gather x1, waiting for transfers between devices, per_device(): value_part = lax.all_gather(value_rows, 'ep', axis=0, tiled=True)  38.8 us
    all_to_all x1, blocking collectives, per_device(): lax.all_to_all(outgoing, 'ep', split_axis=0, concat_axis=0, tiled=True)  33 us
    all_gather x1, waiting for transfers between devices, per_device(): key_part = lax.all_gather(key_rows, 'ep', axis=0, tiled=True)  27.7 us
    all_gather x1, waiting for transfers between devices, per_device(): lax.all_gather(head_out.reshape(1, 1, count_a, head_out.shape[1]), 'tp',...  20.8 us
    reduce_sum x3, other arithmetic, key_block(): new_sum = old_sum * shrink + jnp.sum(weights, axis=-1)  20.5 us
    dot_general x3, matrix products, key_block(): jnp.einsum('ihcd,jhcd->ihcj', query_four, key_four, preferred_element_typ...  20 us
    dot_general x3, matrix products, key_block(): jnp.einsum('ihcj,jhe->ihce', weights.astype(jnp.bfloat16), value_three, p...  10.7 us
  transfers between devices with their start and end apart: 6, of which 5 were waited for; matrix products, arithmetic and copies ran while one was open for 29% of the time, Pallas kernels for 0%

commit v1 on v0

--- a/solution.py
+++ b/solution.py
@@ -66,8 +66,11 @@
         jnp.zeros((count_a, per_head, 2), jnp.float32),
         jnp.zeros((count_a, per_head, 2, value_dim), jnp.float32),
     )
-    key_part = lax.all_gather(key_rows, "ep", axis=0, tiled=True)
-    value_part = lax.all_gather(value_rows, "ep", axis=0, tiled=True)
+    key_part, value_part = jnp.split(
+        lax.all_gather(jnp.concatenate([key_rows, value_rows], axis=1), "ep", axis=0, tiled=True),
+        [key_rows.shape[1]],
+        axis=1,
+    )
     key_count = key_part.shape[0]
 
     def step_block(block_num, inner_state):

time: 288 us -> 288 us (level)
  waiting for transfers between devices: 136 us -> 130 us
  local copies, waits for them, and re-layouts: 21 us -> 25.7 us
    all_to_all x1, waiting for transfers between devices: 0.23 us -> 26.4 us  [per_device(): lax.all_to_all(moe_total.astype(jnp.bfloat16), 'ep', split_axis=0, concat...]
    all_gather x1, waiting for transfers between devices: 20.8 us -> 0.01 us  [per_device(): lax.all_gather(head_out.reshape(1, 1, count_a, head_out.shape[1]), 'tp',...]
    all_gather x2 -> x1, waiting for transfers between devices: 66.5 us -> 55 us  [per_device(): lax.all_gather(jnp.concatenate([key_rows, value_rows], axis=1), 'ep', axi...]
    split x0 -> x1, local copies, waits for them, and re-layouts: none -> 5.88 us  [per_device(): jnp.split(lax.all_gather(jnp.concatenate([key_rows, value_rows], axis=1),...]
  transfers between devices with their start and end apart: 6 -> 5, of which waited for: 5 -> 3; matrix products, arithmetic and copies ran while one was open for 29% -> 31% of each run, Pallas kernels for 0% -> 0%
where the time goes in v1:
time: 288 us
  waiting for transfers between devices  130 us (45%)
  matrix products  50.4 us (18%)
  blocking collectives  33 us (11%)
  other arithmetic  30.3 us (11%)
  local copies, waits for them, and re-layouts  25.7 us (9%)
  between operations  14 us (5%)
  starting transfers between devices  3.9 us (1%)
    all_gather x1, waiting for transfers between devices, per_device(): lax.all_gather(jnp.concatenate([key_rows, value_rows], axis=1), 'ep', axi...  55 us
    all_gather x1, waiting for transfers between devices, per_device(): lax.all_gather(column_parts, 'tp', axis=3, tiled=True)  48.8 us
    all_to_all x1, blocking collectives, per_device(): lax.all_to_all(outgoing, 'ep', split_axis=0, concat_axis=0, tiled=True)  33 us
    all_to_all x1, waiting for transfers between devices, per_device(): lax.all_to_all(moe_total.astype(jnp.bfloat16), 'ep', split_axis=0, concat...  26.4 us
    reduce_sum x3, other arithmetic, key_block(): new_sum = old_sum * shrink + jnp.sum(weights, axis=-1)  20.3 us
    dot_general x3, matrix products, key_block(): jnp.einsum('ihcd,jhcd->ihcj', query_four, key_four, preferred_element_typ...  20 us
    dot_general x3, matrix products, key_block(): jnp.einsum('ihcj,jhe->ihce', weights.astype(jnp.bfloat16), value_three, p...  10.9 us
    dot_general x1, matrix products, per_device(): jnp.einsum('sxcf,xfd->sxcd', lax.all_gather(hidden, 'tp', axis=3, tiled=T...  6.13 us
  transfers between devices with their start and end apart: 5, of which 3 were waited for; matrix products, arithmetic and copies ran while one was open for 31% of the time, Pallas kernels for 0%

profile of v1, /device:TPU:0, one launch (start us, length us, event | category | flops | bytes accessed | tf_op | source)
XLA Modules:
  0.0 287.6 jit_solution(18112408570983247478)
XLA Ops:
  10.2 1.4 scatter_custom_fusion
  12.6 2.1 gather_fusion
  14.7 33.0 %all_to_all.10 = bf16[8,1,64,1024]{3,2,1,0:T(8,128)(2,1)} all-to-all(bf16[8,1,64,1024]{3,2,1,0:T(8,128)(2,1)S(1)} %bitcast.152), channel_id=1, replica_groups=mesh['ep'=8,'tp'=4] {'ep'}, dimensions={0} | all-to-all | bytes 2097152 | tf_op jit(solution)/shard_map/all_to_all | solution.py:111
  49.3 1.2 copy.33
  50.6 48.8 %all-gather.9.cloned.1.call-done = bf16[8,1,64,4096]{3,2,1,0:T(8,128)(2,1)} async-done(((bf16[8,1,64,1024]{3,2,1,0:T(8,128)(2,1)}), bf16[8,1,64,4096]{3,2,1,0:T(8,128)(2,1)}) %all-gather.9.cloned.1.call-update) | async-done | bytes 4194320 | tf_op jit(solution)/shard_map/all_gather | solution.py:112
  99.3 3.2 %fusion.15 = f32[8,64]{1,0:T(8,128)S(1)} fusion(bf16[8,1,64,4096]{3,2,1,0:T(8,128)(2,1)} %all-gather.9.cloned.1.call-done), kind=kLoop, calls=%fused_computation.28 | loop fusion | flops 6290944 | bytes 4196352 | tf_op jit(solution)/shard_map/reduce_sum | solution.py:14
  102.8 4.7 %fusion.43 = f32[8,1,64,512]{3,2,0,1:T(8,128)S(1)} fusion(bf16[1,4096,512]{2,1,0:T(8,128)(2,1)} %param.25, bf16[8,1,64,4096]{3,2,1,0:T(8,128)(2,1)S(1)} %copy-done.1, f32[4096]{0:T(1024)S(1)} %copy-done.8, f32[8,64]{1,0:T(8,128)S(1)} %add_rsqrt_fusion.1), kind=kOutput, calls=%fused_computation.44 | convolution fusion | flops 2155872256 | bytes 9455616 | tf_op jit(solution)/shard_map/sxcd,xdf->sxcf/dot_general | solution.py:113
  107.5 3.3 %fusion.58 = bf16[8,1,64,512]{3,2,0,1:T(8,128)(2,1)} fusion(bf16[1,4096,512]{2,1,0:T(8,128)(2,1)S(1)} %copy-done.7, bf16[8,1,64,4096]{3,2,1,0:T(8,128)(2,1)S(1)} %copy-done.1, f32[4096]{0:T(1024)S(1)} %copy-done.8, f32[8,64]{1,0:T(8,128)S(1)} %add_rsqrt_fusion.1, f32[8,1,64,512]{3,2,0,1:T(8,128)S(1)} %fusion.43), kind=kOutput, calls=%fused_computation.47 | convolution fusion | flops 2157445120 | bytes 9979904 | tf_op jit(solution)/shard_map/sxcd,xdf->sxcf/dot_general | solution.py:116
  111.0 55.0 %all-gather.5.cloned.1.call-done = bf16[3072,1024]{0,1:T(8,128)(2,1)} async-done(((bf16[384,1024]{0,1:T(8,128)(2,1)}), bf16[3072,1024]{0,1:T(8,128)(2,1)}) %all-gather.5.cloned.1.call-update) | async-done | bytes 6291472 | tf_op jit(solution)/shard_map/all_gather | solution.py:70
  166.0 5.9 %fusion.69 = (bf16[3072,512]{0,1:T(8,128)(2,1)}, bf16[3072,512]{0,1:T(8,128)(2,1)}) fusion(bf16[3072,1024]{0,1:T(8,128)(2,1)} %all-gather.5.cloned.1.call-done), kind=kLoop, calls=%fused_computation.77 | loop fusion | bytes 12582912 | tf_op jit(solution)/shard_map/split | solution.py:69
  171.9 62.2 %while.18 = (s32[]{:T(128)}, f32[384,4,2]{0,2,1:T(2,128)S(1)}, f32[384,4,2]{0,2,1:T(2,128)S(1)}, f32[384,4,2,128]{0,3,2,1:T(8,128)S(1)}, bf16[3072,512]{0,1:T(8,...) while((s32[]{:T(128)}, f32[384,4,2]{0,2,1:T(2,128)S(1)}, ...), condition=%wide.region_3.4_spmd.clone, body=%wide.region_0.3_spmd.clone.sunk | while | flops 1250443648 | bytes 99691744 | solution.py:82
  172.2 1.9 constant_dynamic-slice_fusion.3
  174.0 6.7 %fusion.87 = (f32[384,4,2]{0,2,1:T(2,128)S(1)}, f32[4,2,1024,384]{3,2,1,0:T(8,128)}) fusion(pred[384,1024]{0,1:T(8,128)(4,1)S(1)} %broadcast_compare_fusion.2, bf16[1024,4,2,64]{0,3,2,1:T(8,128)(2,1)S(1)} %bitcast.148, bf16[384,4,2,64]{0,3,2,1:T(8,128)(2,1)S(1)} %get-tuple-element.292), kind=kOutput, calls=%fused_computation.6.clone.1 | convolution fusion | flops 412087296 | bytes 14430208 | tf_op jit(solution)/shard_map/while/body/eval_jaxpr/ihcd,jhcd->ihcj/dot_general | solution.py:44
  180.7 6.8 %fusion.89 = f32[384,4,2]{0,2,1:T(2,128)S(1)} fusion(f32[4,2,1024,384]{3,2,1,0:T(8,128)} %get-tuple-element.259, f32[384,4,2]{0,2,1:T(2,128)S(1)} %fusion.88, pred[384,1024]{0,1:T(8,128)(4,1)S(1)} %broadcast_compare_fusion.2), kind=kLoop, calls=%fused_computation.8.clone.1 | loop fusion | flops 15725568 | bytes 13000704 | tf_op jit(solution)/shard_map/while/body/eval_jaxpr/reduce_sum | solution.py:55
  187.6 1.6 copy-done
  189.1 3.6 %bitcast_add_fusion.2 = f32[384,4,2,128]{0,3,2,1:T(8,128)S(1)} fusion(f32[384,4,2,128]{0,3,2,1:T(8,128)S(1)} %get-tuple-element.278, bf16[1024,4,128,1]{0,2,3,1:T(8,128)(2,1)S(1)} %bitcast.149, f32[4,2,1024,384]{3,2,1,0:T(8,128)S(1)} %copy-done, f32[384,4,2]{0,2,1:T(2,128)S(1)} %fusion.88, pred[384,1024]{0,1:T(8,128)(4,1)S(1)} %broadcast_compare_fusion.2, ...), kind=kOutput, calls=%fused_computation.11.clone.1 | convolution fusion | flops 822214656 | bytes 17195008 | tf_op jit(solution)/shard_map/while/body/eval_jaxpr/ihcj,jhe->ihce/dot_general | solution.py:56
  193.1 1.7 constant_dynamic-slice_fusion.3
  194.8 6.7 %fusion.87 = (f32[384,4,2]{0,2,1:T(2,128)S(1)}, f32[4,2,1024,384]{3,2,1,0:T(8,128)}) fusion(pred[384,1024]{0,1:T(8,128)(4,1)S(1)} %broadcast_compare_fusion.2, bf16[1024,4,2,64]{0,3,2,1:T(8,128)(2,1)S(1)} %bitcast.148, bf16[384,4,2,64]{0,3,2,1:T(8,128)(2,1)S(1)} %get-tuple-element.292), kind=kOutput, calls=%fused_computation.6.clone.1 | convolution fusion | flops 412087296 | bytes 14430208 | tf_op jit(solution)/shard_map/while/body/eval_jaxpr/ihcd,jhcd->ihcj/dot_general | solution.py:44
  201.5 6.8 %fusion.89 = f32[384,4,2]{0,2,1:T(2,128)S(1)} fusion(f32[4,2,1024,384]{3,2,1,0:T(8,128)} %get-tuple-element.259, f32[384,4,2]{0,2,1:T(2,128)S(1)} %fusion.88, pred[384,1024]{0,1:T(8,128)(4,1)S(1)} %broadcast_compare_fusion.2), kind=kLoop, calls=%fused_computation.8.clone.1 | loop fusion | flops 15725568 | bytes 13000704 | tf_op jit(solution)/shard_map/while/body/eval_jaxpr/reduce_sum | solution.py:55
  208.3 1.4 copy-done
  209.8 3.6 %bitcast_add_fusion.2 = f32[384,4,2,128]{0,3,2,1:T(8,128)S(1)} fusion(f32[384,4,2,128]{0,3,2,1:T(8,128)S(1)} %get-tuple-element.278, bf16[1024,4,128,1]{0,2,3,1:T(8,128)(2,1)S(1)} %bitcast.149, f32[4,2,1024,384]{3,2,1,0:T(8,128)S(1)} %copy-done, f32[384,4,2]{0,2,1:T(2,128)S(1)} %fusion.88, pred[384,1024]{0,1:T(8,128)(4,1)S(1)} %broadcast_compare_fusion.2, ...), kind=kOutput, calls=%fused_computation.11.clone.1 | convolution fusion | flops 822214656 | bytes 17195008 | tf_op jit(solution)/shard_map/while/body/eval_jaxpr/ihcj,jhe->ihce/dot_general | solution.py:56
  213.8 1.7 constant_dynamic-slice_fusion.3
  215.5 6.7 %fusion.87 = (f32[384,4,2]{0,2,1:T(2,128)S(1)}, f32[4,2,1024,384]{3,2,1,0:T(8,128)}) fusion(pred[384,1024]{0,1:T(8,128)(4,1)S(1)} %broadcast_compare_fusion.2, bf16[1024,4,2,64]{0,3,2,1:T(8,128)(2,1)S(1)} %bitcast.148, bf16[384,4,2,64]{0,3,2,1:T(8,128)(2,1)S(1)} %get-tuple-element.292), kind=kOutput, calls=%fused_computation.6.clone.1 | convolution fusion | flops 412087296 | bytes 14430208 | tf_op jit(solution)/shard_map/while/body/eval_jaxpr/ihcd,jhcd->ihcj/dot_general | solution.py:44
  222.2 6.8 %fusion.89 = f32[384,4,2]{0,2,1:T(2,128)S(1)} fusion(f32[4,2,1024,384]{3,2,1,0:T(8,128)} %get-tuple-element.259, f32[384,4,2]{0,2,1:T(2,128)S(1)} %fusion.88, pred[384,1024]{0,1:T(8,128)(4,1)S(1)} %broadcast_compare_fusion.2), kind=kLoop, calls=%fused_computation.8.clone.1 | loop fusion | flops 15725568 | bytes 13000704 | tf_op jit(solution)/shard_map/while/body/eval_jaxpr/reduce_sum | solution.py:55
  229.0 1.4 copy-done
  230.5 3.6 %bitcast_add_fusion.2 = f32[384,4,2,128]{0,3,2,1:T(8,128)S(1)} fusion(f32[384,4,2,128]{0,3,2,1:T(8,128)S(1)} %get-tuple-element.278, bf16[1024,4,128,1]{0,2,3,1:T(8,128)(2,1)S(1)} %bitcast.149, f32[4,2,1024,384]{3,2,1,0:T(8,128)S(1)} %copy-done, f32[384,4,2]{0,2,1:T(2,128)S(1)} %fusion.88, pred[384,1024]{0,1:T(8,128)(4,1)S(1)} %broadcast_compare_fusion.2, ...), kind=kOutput, calls=%fused_computation.11.clone.1 | convolution fusion | flops 822214656 | bytes 17195008 | tf_op jit(solution)/shard_map/while/body/eval_jaxpr/ihcj,jhe->ihce/dot_general | solution.py:56
  235.7 6.1 %fusion.38 = bf16[8,1,64,1024]{3,2,1,0:T(8,128)(2,1)} fusion(bf16[1,2048,1024]{2,1,0:T(8,128)(2,1)} %param.27, bf16[8,1,64,2048]{3,2,0,1:T(8,128)(2,1)} %all-gather.11.cloned.1.call-done), kind=kOutput, calls=%fused_computation.43 | convolution fusion | flops 2148007936 | bytes 7340032 | tf_op jit(solution)/shard_map/sxcf,xfd->sxcd/dot_general | solution.py:127
  241.8 3.6 %all-to-all-start.1 = ((bf16[8,1,64,1024]{3,2,1,0:T(8,128)(2,1)}), bf16[8,1,64,1024]{3,2,1,0:T(8,128)(2,1)S(1)}, u32[]{:S(2)}, u32[]{:S(2)}) async-start(bf16[8,1,64,1024]{3,2,1,0:T(8,128)(2,1)} %fusion.38), calls=%async_computation.1 | async-start | bytes 2097152 | tf_op jit(solution)/shard_map/all_to_all | solution.py:134
  245.5 26.4 %all-to-all-done.1 = bf16[8,1,64,1024]{3,2,1,0:T(8,128)(2,1)S(1)} async-done(((bf16[8,1,64,1024]{3,2,1,0:T(8,128)(2,1)}), bf16[8,1,64,1024]{3,2,1,0:T(8,128)(2,1)S(1)}, u32[]{:S(2)}, u32[]{:S(2)}) %all-to-all-start.1) | async-done | bytes 1048608 | tf_op jit(solution)/shard_map/all_to_all | solution.py:134
  271.8 1.2 gather_fusion.1
  273.7 2.1 multiply_reduce_fusion
  275.7 5.4 %fusion.35 = bf16[384,1024]{1,0:T(8,128)(2,1)} fusion(bf16[2048,1024]{1,0:T(8,128)(2,1)} %param.20, bf16[1,1,384,2048]{2,3,1,0:T(8,128)(2,1)} %all-gather.7.cloned.1.call-done), kind=kOutput, calls=%fused_computation.42 | convolution fusion | flops 1611005952 | bytes 6553600 | tf_op jit(solution)/shard_map/dot_general | solution.py:119
  (81 shorter events, 9.3 us)
Async XLA Ops:
  7.2 92.2 %all-gather.9.cloned.1.call-start = ((), (), s32[]{:S(2)}) async-start(), calls=%async_computation.4 | async-start | bytes 5242880 | tf_op jit(solution)/shard_map/all_gather | solution.py:112
  12.6 35.1 %copy-start.2 = (bf16[384,512]{1,0:T(8,128)(2,1)S(1)}, bf16[384,512]{1,0:T(8,128)(2,1)}, u32[]{:S(2)}) copy-start(bf16[384,512]{1,0:T(8,128)(2,1)} %param.17) | copy-start | bytes 1179652
  14.7 33.3 %copy-start.3 = (bf16[384,512]{1,0:T(8,128)(2,1)S(1)}, bf16[384,512]{1,0:T(8,128)(2,1)}, u32[]{:S(2)}) copy-start(bf16[384,512]{1,0:T(8,128)(2,1)} %param.16) | copy-start | bytes 1179652
  14.7 35.8 %copy-start.4 = (f32[4]{0:T(128)S(1)}, f32[4]{0:T(128)}, u32[]{:S(2)}) copy-start(f32[4]{0:T(128)} %param.18) | copy-start | bytes 52
  14.7 35.8 %copy-start.6 = (f32[128]{0:T(128)S(1)}, f32[128]{0:T(128)}, u32[]{:S(2)}) copy-start(f32[128]{0:T(128)} %param.19) | copy-start | bytes 1540
  47.7 118.3 %all-gather.5.cloned.1.call-start = ((), (), s32[]{:S(2)}) async-start(), calls=%async_computation.2 | async-start | bytes 7077888 | tf_op jit(solution)/shard_map/all_gather | solution.py:70
  48.0 54.6 %copy-start.8 = (f32[4096]{0:T(1024)S(1)}, f32[4096]{0:T(1024)}, u32[]{:S(2)}) copy-start(f32[4096]{0:T(1024)} %param.22) | copy-start | bytes 49156
  49.2 186.5 %all-gather.11.cloned.1.call-start = ((), (), s32[]{:S(2)}) async-start(), calls=%async_computation.5 | async-start | bytes 2621440 | tf_op jit(solution)/shard_map/all_gather | solution.py:129
  99.3 3.4 %copy-start.1 = (bf16[8,1,64,4096]{3,2,1,0:T(8,128)(2,1)S(1)}, bf16[8,1,64,4096]{3,2,1,0:T(8,128)(2,1)}, u32[]{:S(2)}) copy-start(bf16[8,1,64,4096]{3,2,1,0:T(8,128)(2,1)} %all-gather.9.cloned.1.call-done) | copy-start | bytes 12582916
  102.8 4.7 %copy-start.7 = (bf16[1,4096,512]{2,1,0:T(8,128)(2,1)S(1)}, bf16[1,4096,512]{2,1,0:T(8,128)(2,1)}, u32[]{:S(2)}) copy-start(bf16[1,4096,512]{2,1,0:T(8,128)(2,1)} %param.26) | copy-start | bytes 12582916
  110.8 164.9 %all-gather.7.cloned.1.call-start = ((), (), s32[]{:S(2)}) async-start(), calls=%async_computation.3 | async-start | bytes 1966080 | tf_op jit(solution)/shard_map/all_gather | solution.py:120
  180.7 8.4 %copy-start = (f32[4,2,1024,384]{3,2,1,0:T(8,128)S(1)}, f32[4,2,1024,384]{3,2,1,0:T(8,128)}, u32[]{:S(2)}) copy-start(f32[4,2,1024,384]{3,2,1,0:T(8,128)} %get-tuple-element.259) | copy-start | bytes 37748740 | tf_op jit(solution)/shard_map/while
  201.5 8.3 %copy-start = (f32[4,2,1024,384]{3,2,1,0:T(8,128)S(1)}, f32[4,2,1024,384]{3,2,1,0:T(8,128)}, u32[]{:S(2)}) copy-start(f32[4,2,1024,384]{3,2,1,0:T(8,128)} %get-tuple-element.259) | copy-start | bytes 37748740 | tf_op jit(solution)/shard_map/while
  222.2 8.3 %copy-start = (f32[4,2,1024,384]{3,2,1,0:T(8,128)S(1)}, f32[4,2,1024,384]{3,2,1,0:T(8,128)}, u32[]{:S(2)}) copy-start(f32[4,2,1024,384]{3,2,1,0:T(8,128)} %get-tuple-element.259) | copy-start | bytes 37748740 | tf_op jit(solution)/shard_map/while
  235.6 9.7 %copy-start.5 = (f32[128,2]{0,1:T(2,128)S(1)}, f32[128,2]{0,1:T(2,128)}, u32[]{:S(2)}) copy-start(f32[128,2]{0,1:T(2,128)} %param.24) | copy-start | bytes 3076
  241.8 30.1 %all-to-all-start.1 = ((bf16[8,1,64,1024]{3,2,1,0:T(8,128)(2,1)}), bf16[8,1,64,1024]{3,2,1,0:T(8,128)(2,1)S(1)}, u32[]{:S(2)}, u32[]{:S(2)}) async-start(bf16[8,1,64,1024]{3,2,1,0:T(8,128)(2,1)} %fusion.38), calls=%async_computation.1 | async-start | bytes 2097152 | tf_op jit(solution)/shard_map/all_to_all | solution.py:134
Sparse Core Ops, SparseCore 0:
  47.8 51.4 all-gather.8
  101.5 64.4 all-gather.4
  167.8 33.6 all-gather.10
  235.7 29.1 all-gather.6
